TPU v7x, 32 devices: a whole 2x2x4 slice. The times are simulated.
32 devices in a mesh: grp: 2 (over y), sp: 4 (over z), tp: 4 (over x, core).
Axes of the slice: x: 2, y: 2, z: 4, core: 2. Of those that a mesh axis runs over, the one named last changes fastest.
Arguments:
- tokens: bfloat16 [1280, 2048], P(('grp', 'sp')), parts along dimension 0, may hold values from -6 to 6
- norm_gain: float32 [2048], replicated, may hold values from 0.6 to 5
- query_weight: bfloat16 [2048, 2048], P('sp', 'tp')
- key_weight: bfloat16 [2048, 512], P('sp', 'tp')
- value_weight: bfloat16 [2048, 512], P('sp', 'tp'), may hold values from -0.125 to 0.125
- map_lambda: float32 [16], P('tp'), may hold values from 0.3 to 0.8
- head_gain: float32 [16, 128], P('tp'), may hold values from 0.1 to 1.9
- attn_out_weight: bfloat16 [2048, 2048], P('tp', 'sp'), may hold values from -0.125 to 0.125
- pool_out_weight: bfloat16 [2048, 2048], P('tp', 'sp'), may hold values from -0.09375 to 0.09375
Outputs:
- mixed_rows: bfloat16 [1280, 2048], P(('grp', 'sp', 'tp')), parts along dimension 0
- log_totals: float32 [2, 16, 1280], P(None, 'tp', ('grp', 'sp')), parts along dimension 2
There are 2 independent parts, one for each index of `grp`. A program takes and returns all parts, laid end to end along the dimension named above; an argument that names none is the same for every part. Nothing has to cross between parts.
All inputs are finite; a program needn't handle non-finite values.
Results may differ from a plain program's by a relative error of at most 0.013.
The roundings to bfloat16 on the way count: a program that leaves them out, or rounds other values in their place, can miss the bound.
Values may be sent and summed in bfloat16 or wider, within the bound.
A program may use at most 64 MiB of HBM per device.

v0:
```python
import math

import jax
import jax.numpy as jnp
from jax import lax
from jax.sharding import PartitionSpec as P

HD = 64
VD = 128
POOL_SPAN = 16


epsilon = 1e-06
very_low = -1e30


def extended(cells, sides, width):
    for axis, dim in sides:
        count = lax.axis_size(axis)
        ends = count - 1
        head = lax.slice_in_dim(cells, 0, width, axis=dim)
        tail = lax.slice_in_dim(cells, cells.shape[dim] - width, cells.shape[dim], axis=dim)
        cells = jnp.concatenate(
            [
                lax.ppermute(tail, axis, [(i, (i + 1) % count) for i in range(ends)]),
                cells,
                lax.ppermute(head, axis, [((i + 1) % count, i) for i in range(ends)]),
            ],
            axis=dim,
        )
    return cells


def add_products(totals, pieces, source):
    results = []
    for running, piece in zip(totals, pieces):
        results.append(jnp.dot(source, piece, preferred_element_type=jnp.float32))
    return tuple(results)


def on_device(
    tokens,
    norm_gain,
    query_weight,
    key_weight,
    value_weight,
    map_lambda,
    head_gain,
    attn_out_weight,
    pool_out_weight,
):
    tokens_wide = tokens.astype(jnp.float32)
    normed = (
        tokens_wide
        * lax.rsqrt(jnp.mean(tokens_wide * tokens_wide, axis=-1, keepdims=True) + epsilon)
        * norm_gain
    ).astype(jnp.bfloat16)
    row_count = normed.shape[0]
    sp_index = lax.axis_index("sp")
    tp_index = lax.axis_index("tp")
    group_width = pool_out_weight.shape[0]
    local_heads = map_lambda.shape[0]
    key_heads = value_weight.shape[1] // VD
    group_heads = local_heads // key_heads
    q_empty = jnp.zeros((row_count, query_weight.shape[1]), jnp.float32)
    k_empty = jnp.zeros((row_count, key_weight.shape[1]), jnp.float32)
    v_empty = jnp.zeros((row_count, value_weight.shape[1]), jnp.float32)
    q_acc, k_acc, v_acc = add_products(
        (q_empty, k_empty, v_empty),
        (
            lax.all_gather(query_weight, "sp", axis=0, tiled=True),
            lax.all_gather(key_weight, "sp", axis=0, tiled=True),
            lax.all_gather(value_weight, "sp", axis=0, tiled=True),
        ),
        normed,
    )
    queries = q_acc.astype(jnp.bfloat16).reshape(row_count, key_heads, group_heads, 2, HD)
    keys_flat = k_acc.astype(jnp.bfloat16)
    values_flat = v_acc.astype(jnp.bfloat16)

    def key_block(state_now, key_pair):
        maxima, totals, accums = state_now
        key_blk, val_blk = key_pair
        scores = jnp.einsum(
            "qhgmd,khmd->hgmqk", queries, key_blk, preferred_element_type=jnp.float32
        ) * HD ** (-0.5)
        highest = jnp.maximum(maxima, jnp.max(scores, axis=-1))
        factor = jnp.exp(maxima - highest)
        weights = jnp.exp(scores - highest[..., None])
        totals = totals * factor + jnp.sum(weights, axis=-1)
        accums = accums * factor[..., None] + jnp.einsum(
            "hgmqk,khe->hgmqe",
            weights.astype(jnp.bfloat16),
            val_blk,
            preferred_element_type=jnp.float32,
        )
        return ((highest, totals, accums), None)

    start_state = (
        jnp.full((key_heads, group_heads, 2, row_count), very_low, jnp.float32),
        jnp.zeros((key_heads, group_heads, 2, row_count), jnp.float32),
        jnp.zeros((key_heads, group_heads, 2, row_count, VD), jnp.float32),
    )
    key_piece = lax.all_gather(keys_flat, "sp", axis=0, tiled=True)
    val_piece = lax.all_gather(values_flat, "sp", axis=0, tiled=True)
    piece_len = key_piece.shape[0]
    block_len = math.gcd(piece_len, 512)
    key_blocks = key_piece.reshape(piece_len // block_len, block_len, key_heads, 2, HD)
    val_blocks = val_piece.reshape(piece_len // block_len, block_len, key_heads, VD)
    state_next, unused = lax.scan(key_block, start_state, (key_blocks, val_blocks))
    maxima, totals, accums = state_next
    log_parts = maxima + jnp.log(totals)
    log_totals = jnp.transpose(log_parts, (2, 0, 1, 3)).reshape(2, local_heads, row_count)
    reads = accums / totals[..., None]
    contrast = reads[:, :, 0] - map_lambda.reshape(key_heads, group_heads, 1, 1) * reads[:, :, 1]
    scaled = (
        contrast
        * lax.rsqrt(jnp.mean(contrast * contrast, axis=-1, keepdims=True) + epsilon)
        * head_gain.reshape(key_heads, group_heads, 1, VD)
    )
    attention_head_rows = (
        jnp.transpose(scaled, (2, 0, 1, 3))
        .reshape(row_count, local_heads * VD)
        .astype(jnp.bfloat16)
    )
    head_rows, log_totals = (attention_head_rows, log_totals)
    own_chan = lax.dynamic_slice_in_dim(normed, tp_index * group_width, group_width, 1)
    reach = POOL_SPAN // 2
    padded = extended(own_chan, (("sp", 0),), reach)
    window = jnp.left_shift(jnp.int32(2), tp_index)
    half_span = window // 2
    running = jnp.zeros((row_count, group_width), jnp.float32)
    for offset in range(POOL_SPAN):
        piece = lax.dynamic_slice_in_dim(padded, reach - half_span + offset, row_count, 0).astype(
            jnp.float32
        )
        running = running + jnp.where(offset < window, piece, 0.0)
    seq_len = row_count * lax.axis_size("sp")
    position = sp_index * row_count + jnp.arange(row_count, dtype=jnp.int32)
    lower_edge = jnp.clip(position - half_span, 0, seq_len)
    upper_edge = jnp.clip(position + window - half_span, 0, seq_len)
    counts_f = (upper_edge - lower_edge).astype(jnp.float32)[:, None]
    pooled = (running / counts_f - own_chan.astype(jnp.float32)).astype(jnp.bfloat16)
    attn_whole, pool_whole = (
        lax.all_gather(attn_out_weight, "sp", axis=1, tiled=True),
        lax.all_gather(pool_out_weight, "sp", axis=1, tiled=True),
    )
    mixed = lax.psum_scatter(
        (
            jnp.dot(head_rows, attn_whole, preferred_element_type=jnp.float32)
            + jnp.dot(pooled, pool_whole, preferred_element_type=jnp.float32)
        ).astype(jnp.bfloat16),
        "tp",
        scatter_dimension=0,
        tiled=True,
    )
    return (mixed, log_totals)


def solution(mesh):
    placed = (
        P(("grp", "sp"), None),
        P(),
        P("sp", "tp"),
        P("sp", "tp"),
        P("sp", "tp"),
        P("tp"),
        P("tp", None),
        P("tp", "sp"),
        P("tp", "sp"),
    )
    return jax.shard_map(
        on_device,
        mesh=mesh,
        in_specs=placed,
        out_specs=(P(("grp", "sp", "tp"), None), P(None, "tp", ("grp", "sp"))),
        check_vma=False,
    )
```

profile of v0, /device:TPU:0, one launch (start us, length us, event | category | flops | bytes accessed | tf_op | source)
XLA Modules:
  0.0 200.9 jit_solution(6198464641306412881)
XLA Ops:
  7.2 0.7 all-gather.4.cloned.1.call-update
  8.0 0.7 all-gather.6.cloned.1.call-update
  8.7 1.3 fusion.15
  10.0 1.0 fusion.17
  11.0 5.0 %collective-permute-start = (bf16[8,512]{1,0:T(8,128)(2,1)S(1)}, bf16[8,512]{1,0:T(8,128)(2,1)S(1)}, u32[]{:S(2)}, u32[]{:S(2)}) collective-permute-start(bf16[8,512]{1,0:T(8,128)(2,1)S(1)} %get-tuple-element.102), channel_id=1, source_target_pairs={{0,4},{4,8},{8,12},{1,5},{5,9},{9,13},{2,6},{6,10},{10,14},{3,7},{... | collective-permute-start | bytes 24584 | tf_op jit(solution)/shard_map/ppermute | solution.py:25
  16.0 1.3 collective-permute-start.1
  17.4 24.1 %all_gather.21 = bf16[2048,128]{1,0:T(8,128)(2,1)S(1)} all-gather(bf16[512,128]{1,0:T(8,128)(2,1)S(1)} %copy-done.1), channel_id=1, replica_groups=mesh['grp'=2,'sp'=4,'tp'=4] {'sp'}, dimensions={0}, use_global_device_ids=true | all-gather | bytes 655360 | tf_op jit(solution)/shard_map/all_gather | solution.py:72
  41.9 15.2 %all_gather.22 = bf16[640,128]{1,0:T(8,128)(2,1)S(1)} all-gather(bf16[160,128]{1,0:T(8,128)(2,1)S(1)} %convolution_convert_fusion.2), channel_id=1, replica_groups=mesh['grp'=2,'sp'=4,'tp'=4] {'sp'}, dimensions={0}, use_global_device_ids=true | all-gather | bytes 204800 | tf_op jit(solution)/shard_map/all_gather | solution.py:104
  57.1 21.5 %all_gather.24 = bf16[2048,128]{1,0:T(8,128)(2,1)S(1)} all-gather(bf16[512,128]{1,0:T(8,128)(2,1)S(1)} %copy-done.2), channel_id=1, replica_groups=mesh['grp'=2,'sp'=4,'tp'=4] {'sp'}, dimensions={0}, use_global_device_ids=true | all-gather | bytes 655360 | tf_op jit(solution)/shard_map/all_gather | solution.py:73
  78.9 14.8 %all_gather.25 = bf16[640,128]{1,0:T(8,128)(2,1)S(1)} all-gather(bf16[160,128]{1,0:T(8,128)(2,1)S(1)} %convolution_convert_fusion.1), channel_id=1, replica_groups=mesh['grp'=2,'sp'=4,'tp'=4] {'sp'}, dimensions={0}, use_global_device_ids=true | all-gather | bytes 204800 | tf_op jit(solution)/shard_map/all_gather | solution.py:105
  94.2 2.1 %convolution_convert_fusion = bf16[160,512]{1,0:T(8,128)(2,1)S(1)} fusion(bf16[160,2048]{1,0:T(8,128)(2,1)S(1)} %fusion.17, bf16[2048,512]{1,0:T(8,128)(2,1)} %all-gather.4.cloned.1.call-done), kind=kOutput, calls=%fused_computation.29 | convolution fusion | flops 335626240 | bytes 2916352 | tf_op jit(solution)/shard_map/dot_general | solution.py:37
  96.6 8.5 %while.15 = (s32[]{:T(128)}, f32[1,4,2,160]{3,1,2,0:T(4,128)S(1)}, f32[1,4,2,160]{3,1,2,0:T(4,128)S(1)}, f32[1,4,2,160,128]{4,3,2,1,0:T(8,128)S(1)}, bf16[5,128,...) while((s32[]{:T(128)}, f32[1,4,2,160]{3,1,2,0:T(4,128)S(1)}, ...), condition=%wide.region_4.5_spmd.clone, body=%wide.region_1.4_spmd.clone.sunk | while | flops 64232960 | bytes 3694705 | solution.py:110
  96.6 0.6 fusion.78
  97.2 0.6 fusion.80
  98.3 0.6 fusion.78
  100.0 0.6 fusion.78
  101.7 0.6 fusion.78
  103.4 0.6 fusion.78
  105.9 16.4 %all-gather.6.cloned.1.call-done = bf16[512,2048]{1,0:T(8,128)(2,1)} async-done(((bf16[512,512]{1,0:T(8,128)(2,1)}), bf16[512,2048]{1,0:T(8,128)(2,1)}) %all-gather.6.cloned.1.call-update) | async-done | bytes 2097168 | tf_op jit(solution)/shard_map/all_gather | solution.py:145
  122.4 2.1 %fusion.21 = f32[160,2048]{1,0:T(8,128)S(1)} fusion(bf16[512,2048]{1,0:T(8,128)(2,1)} %all-gather.6.cloned.1.call-done, bf16[20,8,4,128]{3,2,1,0:T(4,128)(2,1)S(1)} %bitcast.102), kind=kOutput, calls=%fused_computation.42 | convolution fusion | flops 335544320 | bytes 3571712 | tf_op jit(solution)/shard_map/dot_general | solution.py:150
  124.5 44.1 %all-gather.8.cloned.1.call-done = bf16[512,2048]{1,0:T(8,128)(2,1)} async-done(((bf16[512,512]{1,0:T(8,128)(2,1)}), bf16[512,2048]{1,0:T(8,128)(2,1)}) %all-gather.8.cloned.1.call-update) | async-done | bytes 2097168 | tf_op jit(solution)/shard_map/all_gather | solution.py:146
  168.6 4.3 %fusion.14 = bf16[160,2048]{1,0:T(8,128)(2,1)} fusion(f32[160,2048]{1,0:T(8,128)S(1)} %fusion.21, bf16[512,2048]{1,0:T(8,128)(2,1)} %all-gather.8.cloned.1.call-done, bf16[160,512]{1,0:T(8,128)(2,1)S(1)} %constant_dynamic-slice_fusion.1, f32[160]{0:T(256)S(1)} %subtract_convert_fusion.2, bf16[176,512]{1,0:T(8,128)(2,1)S(1)} %pad_maximum_fusion, ...), kind=kOutput, calls=%fused_computation.23 | convolution fusion | flops 340377600 | bytes 6849616 | tf_op jit(solution)/shard_map/dot_general | solution.py:151
  172.9 0.6 add_bitcast_fusion
  173.5 20.8 %reduce-scatter.2.cloned.1.call-done = bf16[40,2048]{1,0:T(8,128)(2,1)} async-done(((bf16[160,2048]{1,0:T(8,128)(2,1)}), bf16[40,2048]{1,0:T(8,128)(2,1)}) %reduce-scatter.2.cloned.1.call-update) | async-done | bytes 163856 | tf_op jit(solution)/shard_map/reduce_scatter | solution.py:148
  (68 shorter events, 6.7 us)
Async XLA Ops:
  7.2 2.9 %copy-start = (bf16[160,2048]{1,0:T(8,128)(2,1)S(1)}, bf16[160,2048]{1,0:T(8,128)(2,1)}, u32[]{:S(2)}) copy-start(bf16[160,2048]{1,0:T(8,128)(2,1)} %param.11) | copy-start | bytes 1966084
  7.2 10.3 %copy-start.1 = (bf16[512,128]{1,0:T(8,128)(2,1)S(1)}, bf16[512,128]{1,0:T(8,128)(2,1)}, u32[]{:S(2)}) copy-start(bf16[512,128]{1,0:T(8,128)(2,1)} %param.14) | copy-start | bytes 393220
  7.2 87.0 %all-gather.4.cloned.1.call-start = ((), (), s32[]{:S(2)}) async-start(), calls=%async_computation.1 | async-start | bytes 2621440 | tf_op jit(solution)/shard_map/all_gather | solution.py:71
  7.9 114.4 %all-gather.6.cloned.1.call-start = ((), (), s32[]{:S(2)}) async-start(), calls=%async_computation.2 | async-start | bytes 2621440 | tf_op jit(solution)/shard_map/all_gather | solution.py:145
  8.7 159.9 %all-gather.8.cloned.1.call-start = ((), (), s32[]{:S(2)}) async-start(), calls=%async_computation.3 | async-start | bytes 2621440 | tf_op jit(solution)/shard_map/all_gather | solution.py:146
  10.0 47.0 %copy-start.2 = (bf16[512,128]{1,0:T(8,128)(2,1)S(1)}, bf16[512,128]{1,0:T(8,128)(2,1)}, u32[]{:S(2)}) copy-start(bf16[512,128]{1,0:T(8,128)(2,1)} %param.15) | copy-start | bytes 393220
  11.0 83.1 %collective-permute-start = (bf16[8,512]{1,0:T(8,128)(2,1)S(1)}, bf16[8,512]{1,0:T(8,128)(2,1)S(1)}, u32[]{:S(2)}, u32[]{:S(2)}) collective-permute-start(bf16[8,512]{1,0:T(8,128)(2,1)S(1)} %get-tuple-element.102), channel_id=1, source_target_pairs={{0,4},{4,8},{8,12},{1,5},{5,9},{9,13},{2,6},{6,10},{10,14},{3,7},{... | collective-permute-start | bytes 24584 | tf_op jit(solution)/shard_map/ppermute | solution.py:25
  16.0 78.2 %collective-permute-start.1 = (bf16[8,512]{1,0:T(8,128)(2,1)S(1)}, bf16[8,512]{1,0:T(8,128)(2,1)S(1)}, u32[]{:S(2)}, u32[]{:S(2)}) collective-permute-start(bf16[8,512]{1,0:T(8,128)(2,1)S(1)} %get-tuple-element.103), channel_id=1, source_target_pairs={{4,0},{8,4},{12,8},{5,1},{9,5},{13,9},{6,2},{10,6},{14,10},{7,3},{... | collective-permute-start | bytes 24584 | tf_op jit(solution)/shard_map/ppermute | solution.py:27
  17.3 177.0 %reduce-scatter.2.cloned.1.call-start = ((), (), s32[]{:S(2)}) async-start(), calls=%async_computation.4 | async-start | bytes 819200 | tf_op jit(solution)/shard_map/reduce_scatter | solution.py:148
  96.5 8.8 %copy-start.4 = (f32[4]{0:T(128)S(1)}, f32[4]{0:T(128)}, u32[]{:S(2)}) copy-start(f32[4]{0:T(128)} %param.16) | copy-start | bytes 52
  96.5 9.1 %copy-start.3 = (f32[4,128]{1,0:T(4,128)S(1)}, f32[4,128]{1,0:T(4,128)}, u32[]{:S(2)}) copy-start(f32[4,128]{1,0:T(4,128)} %param.17) | copy-start | bytes 6148
Sparse Core Ops, SparseCore 0:
  9.6 66.0 all-gather.3
  77.3 45.0 all-gather.5
  123.9 44.6 all-gather.7
  173.1 21.2 reduce-scatter.1
where the time goes:
time: 201 us
  waiting for transfers between devices  82.8 us (41%)
  blocking collectives  75.5 us (38%)
  matrix products  14.4 us (7%)
  between operations  14.2 us (7%)
  other arithmetic  6.68 us (3%)
  starting transfers between devices  6.4 us (3%)
    all_gather x1, waiting for transfers between devices, on_device(): lax.all_gather(pool_out_weight, 'sp', axis=1, tiled=True)  44.1 us
    all_gather x1, blocking collectives, on_device(): lax.all_gather(key_weight, 'sp', axis=0, tiled=True)  24.1 us
    all_gather x1, blocking collectives, on_device(): lax.all_gather(value_weight, 'sp', axis=0, tiled=True)  21.5 us
    reduce_scatter x1, waiting for transfers between devices, on_device(): lax.psum_scatter((jnp.dot(head_rows, attn_whole, preferred_element_type=j...  20.8 us
    all_gather x1, waiting for transfers between devices, on_device(): lax.all_gather(attn_out_weight, 'sp', axis=1, tiled=True)  16.4 us
    all_gather x1, blocking collectives, on_device(): key_piece = lax.all_gather(keys_flat, 'sp', axis=0, tiled=True)  15.2 us
    all_gather x1, blocking collectives, on_device(): val_piece = lax.all_gather(values_flat, 'sp', axis=0, tiled=True)  14.8 us
    ppermute x1, starting transfers between devices, extended(): lax.ppermute(tail, axis, [(i, (i + 1) % count) for i in range(ends)])  4.96 us
  transfers between devices with their start and end apart: 6, of which 3 were waited for; matrix products, arithmetic and copies ran while one was open for 9% of the time, Pallas kernels for 0%

commit v1 on v0

--- a/solution.py
+++ b/solution.py
@@ -1,8 +1,11 @@
+import functools
 import math
 
 import jax
 import jax.numpy as jnp
 from jax import lax
+from jax.experimental import pallas as pl
+from jax.experimental.pallas import tpu as pltpu
 from jax.sharding import PartitionSpec as P
 
 HD = 64
@@ -157,6 +160,410 @@
     return (mixed, log_totals)
 
 
+MESH = pl.DeviceIdType.MESH
+LANES = 128
+
+
+def fused_kernel(
+    count,
+    tok,
+    gain,
+    wq,
+    wk,
+    wv,
+    lam,
+    hgain,
+    wao,
+    wpo,
+    mixed_out,
+    lt_out,
+    tok_all,
+    norm_all,
+    w_all,
+    q_all,
+    k_all,
+    v_all,
+    heads_all,
+    pooled_all,
+    part_out,
+    part_in,
+    block_out,
+    block_in,
+    lt_send,
+    lt_in,
+    z_send,
+    z_recv,
+    f_send,
+    f_recv,
+    h_send,
+    h_recv,
+    p_send,
+    p_recv,
+    o_send,
+    o_recv,
+    l_send,
+    l_recv,
+):
+    g = lax.axis_index("grp")
+    s = lax.axis_index("sp")
+    t = lax.axis_index("tp")
+    rows, width = tok.shape
+    quarter = width // 4
+    shard = wq.shape[0]
+    half = shard // 2
+    sib = t + 1 - 2 * lax.rem(t, 2)
+    far = lax.rem(t + 2, 4)
+    diag = lax.rem(sib + 2, 4)
+    twin = 1 - g
+    offs = list(range(1, count))
+    order = sorted(offs, key=lambda o: min(o, count - o))
+    f32, bf16 = jnp.float32, jnp.bfloat16
+
+    def span(index, size):
+        return pl.ds(pl.multiple_of(index * size, size), size)
+
+    def half_rows(owner, part):
+        return pl.ds(pl.multiple_of(owner * shard + part * half, half), half)
+
+    barrier = pltpu.get_barrier_semaphore()
+    for off in offs:
+        pl.semaphore_signal(
+            barrier, inc=1, device_id={"sp": lax.rem(s + off, count)}, device_id_type=MESH
+        )
+    for peer in (sib, far, diag):
+        pl.semaphore_signal(barrier, inc=1, device_id={"tp": peer}, device_id_type=MESH)
+    pl.semaphore_signal(barrier, inc=1, device_id={"grp": twin}, device_id_type=MESH)
+    pl.semaphore_wait(barrier, count - 1 + 4)
+
+    def copy(src, dst, send, recv, where):
+        return pltpu.make_async_remote_copy(
+            src_ref=src,
+            dst_ref=dst,
+            send_sem=send,
+            recv_sem=recv,
+            device_id=where,
+            device_id_type=MESH,
+        )
+
+    def z_copy(kind, off):
+        peer = lax.rem(s + off, count)
+        if kind == 0:
+            src = tok.at[:, span(t, quarter)]
+            dst = tok_all.at[span(s, rows), span(t, quarter)]
+        else:
+            mine = span(g, half)
+            if kind == 1:
+                src, col = wk.at[mine, :], 0
+            elif kind == 2:
+                src, col = wv.at[mine, :], LANES
+            else:
+                src, col = wq.at[mine, span(peer, LANES)], 2 * LANES
+            dst = w_all.at[half_rows(s, g), pl.ds(col, LANES)]
+        return copy(src, dst, z_send.at[kind, off], z_recv.at[kind, off], {"sp": peer})
+
+    def tok_forward(step, off):
+        owner = lax.rem(s + count - off, count)
+        col = span(far if step == 2 else t, quarter)
+        place = tok_all.at[span(owner, rows), col]
+        where = {"tp": far if step == 1 else sib}
+        return copy(place, place, f_send.at[step, off], f_recv.at[step, off], where)
+
+    def w_forward(off):
+        owner = lax.rem(s + count - off, count)
+        place = w_all.at[half_rows(owner, g), :]
+        return copy(place, place, f_send.at[3, off], f_recv.at[3, off], {"grp": twin})
+
+    for kind in range(4):
+        for off in order:
+            z_copy(kind, off).start()
+
+    def norm_block(ref, base, owner):
+        step = 16
+
+        def one(i, carry):
+            x = ref[pl.ds(pl.multiple_of(base + i * step, step), step), :].astype(f32)
+            scale = lax.rsqrt(jnp.mean(x * x, axis=-1, keepdims=True) + epsilon)
+            norm_all[pl.ds(pl.multiple_of(owner * rows + i * step, step), step), :] = (
+                x * scale * gain[...]
+            ).astype(bf16)
+            return carry
+
+        lax.fori_loop(0, rows // step, one, 0)
+
+    w_all[span(s, shard), 0:LANES] = wk[...]
+    w_all[span(s, shard), LANES : 2 * LANES] = wv[...]
+    w_all[span(s, shard), 2 * LANES : 3 * LANES] = wq[:, span(s, LANES)]
+    norm_block(tok, 0, s)
+
+    for off in order:
+        z_copy(0, off).wait_recv()
+        tok_forward(1, off).start()
+        tok_forward(0, off).start()
+    for off in order:
+        tok_forward(1, off).wait_recv()
+        tok_forward(2, off).start()
+    for off in order:
+        tok_forward(0, off).wait_recv()
+        tok_forward(2, off).wait_recv()
+        owner = lax.rem(s + count - off, count)
+        norm_block(tok_all, owner * rows, owner)
+
+    seq = rows * count
+    group = wpo.shape[0]
+    window = jnp.where(t == 0, 2, jnp.where(t == 1, 4, jnp.where(t == 2, 8, 16)))
+    half_span = window // 2
+
+    def pool(b, carry):
+        at = b * rows + lax.broadcasted_iota(jnp.int32, (rows, seq), 0)
+        col = lax.broadcasted_iota(jnp.int32, (rows, seq), 1)
+        inside = (col >= at - half_span) & (col < at + window - half_span)
+        band = jnp.where(inside, 1.0, 0.0).astype(bf16)
+        total = jnp.dot(band, norm_all[:, span(t, group)], preferred_element_type=f32)
+        pos = b * rows + lax.broadcasted_iota(jnp.int32, (rows, 1), 0)
+        low = jnp.maximum(pos - half_span, 0)
+        high = jnp.minimum(pos + window - half_span, seq)
+        own = norm_all[span(b, rows), span(t, group)].astype(f32)
+        pooled_all[span(b, rows), :] = (total / (high - low).astype(f32) - own).astype(bf16)
+        return carry
+
+    for off in order:
+        for kind in (1, 2, 3):
+            z_copy(kind, off).wait_recv()
+        w_forward(off).start()
+    lax.fori_loop(0, count, pool, 0)
+    for off in order:
+        w_forward(off).wait_recv()
+
+    def project(b, carry):
+        acc = jnp.dot(norm_all[span(b, rows), :], w_all[...], preferred_element_type=f32)
+        k_all[span(b, rows), :] = acc[:, 0:LANES].astype(bf16)
+        v_all[span(b, rows), :] = acc[:, LANES : 2 * LANES].astype(bf16)
+        q_all[span(b, rows), :] = acc[:, 2 * LANES : 3 * LANES].astype(bf16)
+        return carry
+
+    lax.fori_loop(0, count, project, 0)
+
+    def head_copy(b, off):
+        place = heads_all.at[span(b, rows), span(s, LANES)]
+        peer = lax.rem(s + off, count)
+        return copy(place, place, h_send.at[b, off], h_recv.at[b, off], {"sp": peer})
+
+    def lt_copy(b):
+        return copy(lt_send.at[b], lt_in.at[s], l_send.at[b], l_recv.at[s], {"sp": b})
+
+    lane = lax.broadcasted_iota(jnp.int32, (rows, LANES), 1)
+    lt_rows = lt_send.shape[2]
+
+    def attend(b, carry):
+        q = q_all[span(b, rows), :]
+        reads, logs = [], []
+        for m in range(2):
+            q_m = jnp.where((lane >= HD) == (m == 1), q, jnp.zeros_like(q))
+            scores = (
+                lax.dot_general(
+                    q_m, k_all[...], (((1,), (1,)), ((), ())), preferred_element_type=f32
+                )
+                * HD ** (-0.5)
+            )
+            highest = jnp.max(scores, axis=-1, keepdims=True)
+            weights = jnp.exp(scores - highest)
+            totals = jnp.sum(weights, axis=-1, keepdims=True)
+            reads.append(
+                jnp.dot(weights.astype(bf16), v_all[...], preferred_element_type=f32) / totals
+            )
+            logs.append(highest + jnp.log(totals))
+        contrast = reads[0] - lam[s] * reads[1]
+        scaled = (
+            contrast
+            * lax.rsqrt(jnp.mean(contrast * contrast, axis=-1, keepdims=True) + epsilon)
+            * hgain[pl.ds(s, 1), :]
+        )
+        heads_all[span(b, rows), span(s, LANES)] = scaled.astype(bf16)
+        for off in order:
+            head_copy(b, off).start()
+        both = jnp.where(lane == 0, logs[0], logs[1])
+        padded = jnp.concatenate([both, jnp.zeros((lt_rows - rows, LANES), f32)], axis=0)
+        lt_send[b] = jnp.transpose(padded)[0:8, :]
+
+        @pl.when(b != s)
+        def _():
+            lt_copy(b).start()
+
+        return carry
+
+    lax.fori_loop(0, count, attend, 0)
+
+    sub = rows // 4
+    peers = (sib, far, diag)
+
+    def part_copy(b, j):
+        return copy(
+            part_out.at[b, peers[j]],
+            part_in.at[b, j],
+            p_send.at[b, j],
+            p_recv.at[b, j],
+            {"tp": peers[j]},
+        )
+
+    def outward(b, carry):
+        for off in order:
+            head_copy(b, off).wait_recv()
+        total = jnp.dot(heads_all[span(b, rows), :], wao[...], preferred_element_type=f32)
+        total = total + jnp.dot(
+            pooled_all[span(b, rows), :], wpo[...], preferred_element_type=f32
+        )
+        for j in range(4):
+            part_out[b, j] = total[j * sub : (j + 1) * sub, :].astype(bf16)
+        for j in (2, 1, 0):
+            part_copy(b, j).start()
+        return carry
+
+    lax.fori_loop(0, count, outward, 0)
+
+    def out_copy(b):
+        return copy(block_out.at[b], block_in.at[s], o_send.at[b], o_recv.at[s], {"sp": b})
+
+    def finish(b, carry):
+        total = part_out[b, t].astype(f32)
+        for j in range(3):
+            part_copy(b, j).wait_recv()
+            total = total + part_in[b, j].astype(f32)
+        block_out[b] = total.astype(bf16)
+
+        @pl.when(b != s)
+        def _():
+            out_copy(b).start()
+
+        return carry
+
+    lax.fori_loop(0, count, finish, 0)
+    for b in range(count):
+        cols = slice(b * group, (b + 1) * group)
+
+        @pl.when(s == b)
+        def _():
+            mixed_out[:, cols] = block_out[b]
+            lt_out[b] = lt_send[b]
+
+        @pl.when(s != b)
+        def _():
+            copy(
+                block_out.at[s], block_in.at[b], o_send.at[s], o_recv.at[b], {"sp": b}
+            ).wait_recv()
+            copy(lt_send.at[s], lt_in.at[b], l_send.at[s], l_recv.at[b], {"sp": b}).wait_recv()
+            mixed_out[:, cols] = block_in[b]
+            lt_out[b] = lt_in[b]
+            out_copy(b).wait_send()
+            lt_copy(b).wait_send()
+
+    for off in order:
+        for kind in range(4):
+            z_copy(kind, off).wait_send()
+        for step in range(3):
+            tok_forward(step, off).wait_send()
+        w_forward(off).wait_send()
+
+    def drain(b, carry):
+        for off in order:
+            head_copy(b, off).wait_send()
+        for j in range(3):
+            part_copy(b, j).wait_send()
+        return carry
+
+    lax.fori_loop(0, count, drain, 0)
+
+
+def fused(
+    count,
+    tokens,
+    norm_gain,
+    query_weight,
+    key_weight,
+    value_weight,
+    map_lambda,
+    head_gain,
+    attn_out_weight,
+    pool_out_weight,
+):
+    rows, width = tokens.shape
+    cols = attn_out_weight.shape[1]
+    sub = rows // 4
+    seq = rows * count
+    lt_rows = -(-rows // LANES) * LANES
+    bf16, f32 = jnp.bfloat16, jnp.float32
+    vmem = pl.BlockSpec(memory_space=pltpu.VMEM)
+    smem = pl.BlockSpec(memory_space=pltpu.SMEM)
+    sems = pltpu.SemaphoreType.DMA
+    mixed, logs = pl.pallas_call(
+        functools.partial(fused_kernel, count),
+        out_shape=(
+            jax.ShapeDtypeStruct((sub, width), bf16),
+            jax.ShapeDtypeStruct((count, 8, lt_rows), f32),
+        ),
+        in_specs=[vmem] * 5 + [smem] + [vmem] * 3,
+        out_specs=(vmem, vmem),
+        scratch_shapes=[
+            pltpu.VMEM((seq, width), bf16),
+            pltpu.VMEM((seq, width), bf16),
+            pltpu.VMEM((width, 3 * LANES), bf16),
+            pltpu.VMEM((seq, LANES), bf16),
+            pltpu.VMEM((seq, LANES), bf16),
+            pltpu.VMEM((seq, LANES), bf16),
+            pltpu.VMEM((seq, count * LANES), bf16),
+            pltpu.VMEM((seq, pool_out_weight.shape[0]), bf16),
+            pltpu.VMEM((count, 4, sub, cols), bf16),
+            pltpu.VMEM((count, 3, sub, cols), bf16),
+            pltpu.VMEM((count, sub, cols), bf16),
+            pltpu.VMEM((count, sub, cols), bf16),
+            pltpu.VMEM((count, 8, lt_rows), f32),
+            pltpu.VMEM((count, 8, lt_rows), f32),
+            sems((4, count)),
+            sems((4, count)),
+            sems((4, count)),
+            sems((4, count)),
+            sems((count, count)),
+            sems((count, count)),
+            sems((count, 3)),
+            sems((count, 3)),
+            sems((count,)),
+            sems((count,)),
+            sems((count,)),
+            sems((count,)),
+        ],
+        compiler_params=pltpu.CompilerParams(collective_id=0, has_side_effects=True),
+    )(
+        tokens,
+        norm_gain.reshape(1, width),
+        query_weight,
+        key_weight,
+        value_weight,
+        map_lambda,
+        head_gain,
+        attn_out_weight,
+        pool_out_weight,
+    )
+    return mixed, jnp.transpose(logs[:, 0:2, 0:rows], (1, 0, 2))
+
+
+def fits(shape, tokens, query_weight, value_weight, map_lambda, pool_out_weight):
+    count = shape["sp"]
+    return (
+        shape["grp"] == 2
+        and shape["tp"] == 4
+        and count > 1
+        and map_lambda.shape[0] == count
+        and value_weight.shape[1] == VD == LANES == 2 * HD
+        and tokens.shape[0] % 32 == 0
+        and tokens.shape[1] % (4 * LANES) == 0
+        and query_weight.shape[0] % 32 == 0
+        and pool_out_weight.shape[0] * 4 == tokens.shape[1]
+        and pool_out_weight.shape[1] % LANES == 0
+        and pool_out_weight.shape[1] * count == tokens.shape[1]
+        and pool_out_weight.shape[0] == pool_out_weight.shape[1]
+        and tokens.shape[0] * count * tokens.shape[1] <= 1 << 22
+    )
+
+
 def solution(mesh):
     placed = (
         P(("grp", "sp"), None),
@@ -169,8 +576,15 @@
         P("tp", "sp"),
         P("tp", "sp"),
     )
+    shape = dict(mesh.shape)
+
+    def chosen(*args):
+        if fits(shape, args[0], args[2], args[4], args[5], args[8]):
+            return fused(shape["sp"], *args)
+        return on_device(*args)
+
     return jax.shard_map(
-        on_device,
+        chosen,
         mesh=mesh,
         in_specs=placed,
         out_specs=(P(("grp", "sp", "tp"), None), P(None, "tp", ("grp", "sp"))),

time: 201 us -> 82.8 us (0.41)
  waiting for transfers between devices: 82.8 us -> 0 us
  Pallas kernels: 0 us -> 79 us
  blocking collectives: 75.5 us -> 0 us
  matrix products: 14.4 us -> 0 us
  between operations: 14.2 us -> 0.64 us
  other arithmetic: 6.68 us -> 0 us
  starting transfers between devices: 6.4 us -> 0 us
  local copies, waits for them, and re-layouts: 0.68 us -> 2.96 us
    pallas_call x0 -> x1, Pallas kernels: none -> 79 us  [fused(): pl.pallas_call(functools.partial(fused_kernel, count), out_shape=(jax.Sha...]
    all_gather x4 -> x0, blocking collectives: 75.5 us -> none  [the longest x1 24.1 us: on_device(): lax.all_gather(key_weight, 'sp', axis=0, tiled=True)]
    all_gather x3 -> x0, waiting for transfers between devices: 60.6 us -> none  [the longest x1 44.1 us: on_device(): lax.all_gather(pool_out_weight, 'sp', axis=1, tiled=True)]
    reduce_scatter x1 -> x0, waiting for transfers between devices: 20.8 us -> none  [on_device(): lax.psum_scatter((jnp.dot(head_rows, attn_whole, preferred_element_type=j...]
    dot_general x15 -> x0, matrix products: 14.4 us -> none  [the longest x1 4.33 us: on_device(): jnp.dot(pooled, pool_whole, preferred_element_type=jnp.float32)]
    ppermute x2 -> x0, starting transfers between devices: 6.25 us -> none  [the longest x1 4.96 us: extended(): lax.ppermute(tail, axis, [(i, (i + 1) % count) for i in range(ends)])]
    another operation x5 -> x0, other arithmetic: 2.92 us -> none
  transfers between devices with their start and end apart: 6 -> 0, of which waited for: 3 -> 0; matrix products, arithmetic and copies ran while one was open for 9% -> 0% of each run, Pallas kernels for 0% -> 0%
where the time goes in v1:
time: 82.8 us; the launch traced here: 82.6 us
  Pallas kernels  79 us (95%)
  local copies, waits for them, and re-layouts  2.96 us (4%)
    pallas_call x1, Pallas kernels, fused(): pl.pallas_call(functools.partial(fused_kernel, count), out_shape=(jax.Sha...  79 us
    unnamed x2, local copies, waits for them, and re-layouts  2.19 us

profile of v1, /device:TPU:0, one launch (start us, length us, event | category | flops | bytes accessed | tf_op | source)
XLA Modules:
  0.0 82.6 jit_solution(8737987865114409416)
XLA Ops:
  0.6 79.0 %shard_map.104 = (bf16[40,2048]{1,0:T(8,128)(2,1)}, f32[4,8,256]{2,1,0:T(8,128)}) custom-call(bf16[160,2048]{1,0:T(8,128)(2,1)} %tok.1, f32[1,2048]{1,0:T(1,128)} %bitcast.3, bf16[512,512]{1,0:T(8,128)(2,1)} %wq.1, bf16[512,128]{1,0:T(8,128)(2,1)} %wk.1, bf16[512,128]{1,0:T(8,128)(2,1)} %wv.1, f32[4]{0:T(128)} %lam.1, f32[4,128]{1,0:T(4,128)} %hgain.1, ...), custom_call_target="tpu_custom_call" | custom-call | tf_op jit(solution)/shard_map/pallas_call | solution.py:497
  79.6 0.8 slice_bitcast_fusion
  80.4 0.6 copy.11
  81.0 1.6 %copy.13 = bf16[40,2048]{1,0:T(8,128)(2,1)} copy(bf16[40,2048]{1,0:T(8,128)(2,1)} %get-tuple-element.10) | data formatting | bytes 327680

commit v2 on v1

--- a/solution.py
+++ b/solution.py
@@ -191,6 +191,11 @@
     block_in,
     lt_send,
     lt_in,
+    wao_in,
+    wpo_in,
+    local_sem,
+    q_send,
+    q_recv,
     z_send,
     z_recv,
     f_send,
@@ -225,6 +230,19 @@
     def half_rows(owner, part):
         return pl.ds(pl.multiple_of(owner * shard + part * half, half), half)
 
+    pieces = (
+        (tok, tok_all.at[span(s, rows), :]),
+        (wk, w_all.at[span(s, shard), 0:LANES]),
+        (wv, w_all.at[span(s, shard), LANES : 2 * LANES]),
+        (wq.at[:, span(s, LANES)], w_all.at[span(s, shard), 2 * LANES : 3 * LANES]),
+        (wao, wao_in),
+        (wpo, wpo_in),
+    )
+    local = [
+        pltpu.make_async_copy(src, dst, local_sem.at[i]) for i, (src, dst) in enumerate(pieces)
+    ]
+    for piece in local:
+        piece.start()
     barrier = pltpu.get_barrier_semaphore()
     for off in offs:
         pl.semaphore_signal(
@@ -245,68 +263,125 @@
             device_id_type=MESH,
         )
 
-    def z_copy(kind, off):
+    kv = slice(0, 2 * LANES)
+    qs = slice(2 * LANES, 3 * LANES)
+
+    def z_copy(kind, owner, up):
+        if kind == 0:
+            place = tok_all.at[span(owner, rows), span(t, quarter)]
+        else:
+            place = w_all.at[half_rows(owner, g), kv]
+        step = 1 if up else -1
+        return copy(
+            place,
+            place,
+            z_send.at[kind, owner, int(up)],
+            z_recv.at[kind, owner],
+            {"sp": lax.rem(s + step + count, count)},
+        )
+
+    def q_copy(off):
         peer = lax.rem(s + off, count)
-        if kind == 0:
-            src = tok.at[:, span(t, quarter)]
-            dst = tok_all.at[span(s, rows), span(t, quarter)]
-        else:
-            mine = span(g, half)
-            if kind == 1:
-                src, col = wk.at[mine, :], 0
-            elif kind == 2:
-                src, col = wv.at[mine, :], LANES
-            else:
-                src, col = wq.at[mine, span(peer, LANES)], 2 * LANES
-            dst = w_all.at[half_rows(s, g), pl.ds(col, LANES)]
-        return copy(src, dst, z_send.at[kind, off], z_recv.at[kind, off], {"sp": peer})
-
-    def tok_forward(step, off):
-        owner = lax.rem(s + count - off, count)
+        src = wq.at[span(g, half), span(peer, LANES)]
+        dst = w_all.at[half_rows(s, g), qs]
+        return copy(src, dst, q_send.at[off], q_recv.at[s], {"sp": peer})
+
+    def q_arrival(owner):
+        place = w_all.at[half_rows(owner, g), qs]
+        return copy(place, place, q_send.at[0], q_recv.at[owner], {"sp": owner})
+
+    def tok_forward(step, owner):
         col = span(far if step == 2 else t, quarter)
         place = tok_all.at[span(owner, rows), col]
         where = {"tp": far if step == 1 else sib}
-        return copy(place, place, f_send.at[step, off], f_recv.at[step, off], where)
-
-    def w_forward(off):
-        owner = lax.rem(s + count - off, count)
-        place = w_all.at[half_rows(owner, g), :]
-        return copy(place, place, f_send.at[3, off], f_recv.at[3, off], {"grp": twin})
-
-    for kind in range(4):
-        for off in order:
-            z_copy(kind, off).start()
-
-    def norm_block(ref, base, owner):
+        return copy(place, place, f_send.at[step, owner], f_recv.at[step, owner], where)
+
+    def w_forward(kind, owner):
+        place = w_all.at[half_rows(owner, g), qs if kind else kv]
+        at = 3 + kind
+        return copy(place, place, f_send.at[at, owner], f_recv.at[at, owner], {"grp": twin})
+
+    def sides(k, act):
+        @pl.when(s >= k)
+        def _():
+            act(s - k, True, s < count - 1)
+
+        @pl.when(s + k < count)
+        def _():
+            act(s + k, False, s > 0)
+
+    def both_ways(act):
+        @pl.when(s < count - 1)
+        def _():
+            act(True)
+
+        @pl.when(s > 0)
+        def _():
+            act(False)
+
+    local[0].wait()
+    both_ways(lambda up: z_copy(0, s, up).start())
+    local[1].wait()
+    local[2].wait()
+    both_ways(lambda up: z_copy(1, s, up).start())
+    for off in order:
+        q_copy(off).start()
+
+    def norm_block(owner):
         step = 16
 
         def one(i, carry):
-            x = ref[pl.ds(pl.multiple_of(base + i * step, step), step), :].astype(f32)
+            at = pl.ds(pl.multiple_of(owner * rows + i * step, step), step)
+            x = tok_all[at, :].astype(f32)
             scale = lax.rsqrt(jnp.mean(x * x, axis=-1, keepdims=True) + epsilon)
-            norm_all[pl.ds(pl.multiple_of(owner * rows + i * step, step), step), :] = (
-                x * scale * gain[...]
-            ).astype(bf16)
+            norm_all[at, :] = (x * scale * gain[...]).astype(bf16)
             return carry
 
         lax.fori_loop(0, rows // step, one, 0)
 
-    w_all[span(s, shard), 0:LANES] = wk[...]
-    w_all[span(s, shard), LANES : 2 * LANES] = wv[...]
-    w_all[span(s, shard), 2 * LANES : 3 * LANES] = wq[:, span(s, LANES)]
-    norm_block(tok, 0, s)
-
-    for off in order:
-        z_copy(0, off).wait_recv()
-        tok_forward(1, off).start()
-        tok_forward(0, off).start()
-    for off in order:
-        tok_forward(1, off).wait_recv()
-        tok_forward(2, off).start()
-    for off in order:
-        tok_forward(0, off).wait_recv()
-        tok_forward(2, off).wait_recv()
-        owner = lax.rem(s + count - off, count)
-        norm_block(tok_all, owner * rows, owner)
+    def z_tok(owner, up, more):
+        z_copy(0, owner, True).wait_recv()
+
+        @pl.when(more)
+        def _():
+            z_copy(0, owner, up).start()
+
+        tok_forward(1, owner).start()
+        tok_forward(0, owner).start()
+
+    def z_weight(owner, up, more):
+        z_copy(1, owner, True).wait_recv()
+
+        @pl.when(more)
+        def _():
+            z_copy(1, owner, up).start()
+
+        w_forward(0, owner).start()
+        q_arrival(owner).wait_recv()
+        w_forward(1, owner).start()
+
+    def x_tok(owner, up, more):
+        tok_forward(1, owner).wait_recv()
+        tok_forward(2, owner).start()
+
+    def norm_owner(owner, up, more):
+        tok_forward(0, owner).wait_recv()
+        tok_forward(2, owner).wait_recv()
+        norm_block(owner)
+
+    norm_block(s)
+    last = count - 1
+    for k in range(1, count):
+        sides(k, z_tok)
+        if k > 1:
+            sides(k - 1, x_tok)
+        if k > 2:
+            sides(k - 2, norm_owner)
+        sides(k, z_weight)
+    if last > 1:
+        sides(last - 1, norm_owner)
+    sides(last, x_tok)
+    sides(last, norm_owner)
 
     seq = rows * count
     group = wpo.shape[0]
@@ -326,13 +401,15 @@
         pooled_all[span(b, rows), :] = (total / (high - low).astype(f32) - own).astype(bf16)
         return carry
 
-    for off in order:
-        for kind in (1, 2, 3):
-            z_copy(kind, off).wait_recv()
-        w_forward(off).start()
     lax.fori_loop(0, count, pool, 0)
-    for off in order:
-        w_forward(off).wait_recv()
+
+    def y_arrival(owner, up, more):
+        w_forward(0, owner).wait_recv()
+        w_forward(1, owner).wait_recv()
+
+    for k in range(1, count):
+        sides(k, y_arrival)
+    local[3].wait()
 
     def project(b, carry):
         acc = jnp.dot(norm_all[span(b, rows), :], w_all[...], preferred_element_type=f32)
@@ -405,12 +482,15 @@
             {"tp": peers[j]},
         )
 
+    local[4].wait()
+    local[5].wait()
+
     def outward(b, carry):
         for off in order:
             head_copy(b, off).wait_recv()
-        total = jnp.dot(heads_all[span(b, rows), :], wao[...], preferred_element_type=f32)
+        total = jnp.dot(heads_all[span(b, rows), :], wao_in[...], preferred_element_type=f32)
         total = total + jnp.dot(
-            pooled_all[span(b, rows), :], wpo[...], preferred_element_type=f32
+            pooled_all[span(b, rows), :], wpo_in[...], preferred_element_type=f32
         )
         for j in range(4):
             part_out[b, j] = total[j * sub : (j + 1) * sub, :].astype(bf16)
@@ -456,12 +536,24 @@
             out_copy(b).wait_send()
             lt_copy(b).wait_send()
 
+    both_ways(lambda up: z_copy(0, s, up).wait_send())
+    both_ways(lambda up: z_copy(1, s, up).wait_send())
     for off in order:
-        for kind in range(4):
-            z_copy(kind, off).wait_send()
+        q_copy(off).wait_send()
+
+    def sent(owner, up, more):
+        @pl.when(more)
+        def _():
+            z_copy(0, owner, up).wait_send()
+            z_copy(1, owner, up).wait_send()
+
         for step in range(3):
-            tok_forward(step, off).wait_send()
-        w_forward(off).wait_send()
+            tok_forward(step, owner).wait_send()
+        w_forward(0, owner).wait_send()
+        w_forward(1, owner).wait_send()
+
+    for k in range(1, count):
+        sides(k, sent)
 
     def drain(b, carry):
         for off in order:
@@ -493,6 +585,7 @@
     bf16, f32 = jnp.bfloat16, jnp.float32
     vmem = pl.BlockSpec(memory_space=pltpu.VMEM)
     smem = pl.BlockSpec(memory_space=pltpu.SMEM)
+    far = pl.BlockSpec(memory_space=pl.ANY)
     sems = pltpu.SemaphoreType.DMA
     mixed, logs = pl.pallas_call(
         functools.partial(fused_kernel, count),
@@ -500,7 +593,7 @@
             jax.ShapeDtypeStruct((sub, width), bf16),
             jax.ShapeDtypeStruct((count, 8, lt_rows), f32),
         ),
-        in_specs=[vmem] * 5 + [smem] + [vmem] * 3,
+        in_specs=[far, vmem, far, far, far, smem, vmem, far, far],
         out_specs=(vmem, vmem),
         scratch_shapes=[
             pltpu.VMEM((seq, width), bf16),
@@ -517,10 +610,15 @@
             pltpu.VMEM((count, sub, cols), bf16),
             pltpu.VMEM((count, 8, lt_rows), f32),
             pltpu.VMEM((count, 8, lt_rows), f32),
-            sems((4, count)),
-            sems((4, count)),
-            sems((4, count)),
-            sems((4, count)),
+            pltpu.VMEM(attn_out_weight.shape, bf16),
+            pltpu.VMEM(pool_out_weight.shape, bf16),
+            sems((6,)),
+            sems((count,)),
+            sems((count,)),
+            sems((2, count, 2)),
+            sems((2, count)),
+            sems((5, count)),
+            sems((5, count)),
             sems((count, count)),
             sems((count, count)),
             sems((count, 3)),

time: 82.8 us -> 64.4 us (0.78)
  Pallas kernels: 79 us -> 60.6 us
    pallas_call x1, Pallas kernels: 79 us -> 60.6 us  [fused(): pl.pallas_call(functools.partial(fused_kernel, count), out_shape=(jax.Sha...]
where the time goes in v2:
time: 64.4 us; the launch traced here: 64.2 us
  Pallas kernels  60.6 us (94%)
  local copies, waits for them, and re-layouts  2.96 us (5%)
    pallas_call x1, Pallas kernels, fused(): pl.pallas_call(functools.partial(fused_kernel, count), out_shape=(jax.Sha...  60.6 us
    unnamed x2, local copies, waits for them, and re-layouts  2.19 us

profile of v2, /device:TPU:0, one launch (start us, length us, event | category | flops | bytes accessed | tf_op | source)
XLA Modules:
  0.0 64.2 jit_solution(10465903612025374651)
XLA Ops:
  0.6 60.6 %shard_map.104 = (bf16[40,2048]{1,0:T(8,128)(2,1)}, f32[4,8,256]{2,1,0:T(8,128)}) custom-call(bf16[160,2048]{1,0:T(8,128)(2,1)} %tok.1, f32[1,2048]{1,0:T(1,128)} %bitcast.3, bf16[512,512]{1,0:T(8,128)(2,1)} %wq.1, bf16[512,128]{1,0:T(8,128)(2,1)} %wk.1, bf16[512,128]{1,0:T(8,128)(2,1)} %wv.1, f32[4]{0:T(128)} %lam.1, f32[4,128]{1,0:T(4,128)} %hgain.1, ...), custom_call_target="tpu_custom_call" | custom-call | tf_op jit(solution)/shard_map/pallas_call | solution.py:590
  61.2 0.8 %slice_bitcast_fusion = f32[2,4,160]{2,0,1:T(2,128)S(1)} fusion(f32[4,8,256]{2,1,0:T(8,128)} %get-tuple-element.5), kind=kLoop, calls=%fused_computation | loop fusion | bytes 10240 | tf_op jit(solution)/shard_map/transpose | solution.py:643
  62.0 0.6 copy.11
  62.6 1.6 %copy.13 = bf16[40,2048]{1,0:T(8,128)(2,1)} copy(bf16[40,2048]{1,0:T(8,128)(2,1)} %get-tuple-element.10) | data formatting | bytes 327680

commit v3 on v2

--- a/solution.py
+++ b/solution.py
@@ -485,6 +485,20 @@
     local[4].wait()
     local[5].wait()
 
+    def out_copy(b):
+        return copy(block_out.at[b], block_in.at[s], o_send.at[b], o_recv.at[s], {"sp": b})
+
+    def finish(b):
+        total = part_out[b, t].astype(f32)
+        for j in range(3):
+            part_copy(b, j).wait_recv()
+            total = total + part_in[b, j].astype(f32)
+        block_out[b] = total.astype(bf16)
+
+        @pl.when(b != s)
+        def _():
+            out_copy(b).start()
+
     def outward(b, carry):
         for off in order:
             head_copy(b, off).wait_recv()
@@ -496,34 +510,28 @@
             part_out[b, j] = total[j * sub : (j + 1) * sub, :].astype(bf16)
         for j in (2, 1, 0):
             part_copy(b, j).start()
+
+        @pl.when(b > 0)
+        def _():
+            finish(b - 1)
+
         return carry
 
     lax.fori_loop(0, count, outward, 0)
 
-    def out_copy(b):
-        return copy(block_out.at[b], block_in.at[s], o_send.at[b], o_recv.at[s], {"sp": b})
-
-    def finish(b, carry):
-        total = part_out[b, t].astype(f32)
-        for j in range(3):
-            part_copy(b, j).wait_recv()
-            total = total + part_in[b, j].astype(f32)
-        block_out[b] = total.astype(bf16)
-
-        @pl.when(b != s)
-        def _():
-            out_copy(b).start()
-
-        return carry
-
-    lax.fori_loop(0, count, finish, 0)
+    finish(count - 1)
+
+    def put_logs(b, ref):
+        for m in range(2):
+            lt_out[m, b : b + 1, :] = ref[b, m : m + 1, 0:rows]
+
     for b in range(count):
         cols = slice(b * group, (b + 1) * group)
 
         @pl.when(s == b)
         def _():
             mixed_out[:, cols] = block_out[b]
-            lt_out[b] = lt_send[b]
+            put_logs(b, lt_send)
 
         @pl.when(s != b)
         def _():
@@ -532,7 +540,7 @@
             ).wait_recv()
             copy(lt_send.at[s], lt_in.at[b], l_send.at[s], l_recv.at[b], {"sp": b}).wait_recv()
             mixed_out[:, cols] = block_in[b]
-            lt_out[b] = lt_in[b]
+            put_logs(b, lt_in)
             out_copy(b).wait_send()
             lt_copy(b).wait_send()
 
@@ -587,11 +595,11 @@
     smem = pl.BlockSpec(memory_space=pltpu.SMEM)
     far = pl.BlockSpec(memory_space=pl.ANY)
     sems = pltpu.SemaphoreType.DMA
-    mixed, logs = pl.pallas_call(
+    return pl.pallas_call(
         functools.partial(fused_kernel, count),
         out_shape=(
             jax.ShapeDtypeStruct((sub, width), bf16),
-            jax.ShapeDtypeStruct((count, 8, lt_rows), f32),
+            jax.ShapeDtypeStruct((2, count, rows), f32),
         ),
         in_specs=[far, vmem, far, far, far, smem, vmem, far, far],
         out_specs=(vmem, vmem),
@@ -640,7 +648,6 @@
         attn_out_weight,
         pool_out_weight,
     )
-    return mixed, jnp.transpose(logs[:, 0:2, 0:rows], (1, 0, 2))
 
 
 def fits(shape, tokens, query_weight, value_weight, map_lambda, pool_out_weight):

time: 64.4 us -> 63.1 us (0.980)
  local copies, waits for them, and re-layouts: 2.96 us -> 2.2 us
  Pallas kernels: 60.6 us -> 59.9 us
    transpose x1 -> x0, local copies, waits for them, and re-layouts: 0.76 us -> none  [fused(): return (mixed, jnp.transpose(logs[:, 0:2, 0:rows], (1, 0, 2)))]
    unnamed x2 -> x4, local copies, waits for them, and re-layouts: 2.19 us -> 2.2 us
where the time goes in v3:
time: 63.1 us; the launch traced here: 62.8 us
  Pallas kernels  59.9 us (95%)
  local copies, waits for them, and re-layouts  2.2 us (3%)
  between operations  0.65 us (1%)
    pallas_call x1, Pallas kernels, fused(): pl.pallas_call(functools.partial(fused_kernel, count), out_shape=(jax.Sha...  59.9 us
    unnamed x4, local copies, waits for them, and re-layouts  2.2 us

profile of v3, /device:TPU:0, one launch (start us, length us, event | category | flops | bytes accessed | tf_op | source)
XLA Modules:
  0.0 62.8 jit_solution(9898441131046670579)
XLA Ops:
  0.6 59.9 %shard_map.104 = (bf16[40,2048]{1,0:T(8,128)(2,1)}, f32[2,4,160]{2,1,0:T(4,128)}) custom-call(bf16[160,2048]{1,0:T(8,128)(2,1)} %tok.1, f32[1,2048]{1,0:T(1,128)} %bitcast.1, bf16[512,512]{1,0:T(8,128)(2,1)} %wq.1, bf16[512,128]{1,0:T(8,128)(2,1)} %wk.1, bf16[512,128]{1,0:T(8,128)(2,1)} %wv.1, f32[4]{0:T(128)} %lam.1, f32[4,128]{1,0:T(4,128)} %hgain.1, ...), custom_call_target="tpu_custom_call" | custom-call | tf_op jit(solution)/shard_map/pallas_call | solution.py:598
  60.6 0.0 copy-start
  60.6 1.6 %copy.13 = bf16[40,2048]{1,0:T(8,128)(2,1)} copy(bf16[40,2048]{1,0:T(8,128)(2,1)} %get-tuple-element.4) | data formatting | bytes 327680
  62.2 0.0 copy-done
  62.2 0.6 copy.14
Async XLA Ops:
  60.6 1.6 %copy-start = (f32[2,4,160]{2,1,0:T(4,128)S(1)}, f32[2,4,160]{2,1,0:T(4,128)}, u32[]{:S(2)}) copy-start(f32[2,4,160]{2,1,0:T(4,128)} %get-tuple-element.5) | copy-start | bytes 15364
